TPU v7x, 32 devices: a whole 2x2x4 slice. The times are simulated.
32 devices in a mesh: sp: 8 (over z, y), tp: 4 (over x, core).
Axes of the slice: x: 2, y: 2, z: 4, core: 2. Of those that a mesh axis runs over, the one named last changes fastest.
Arguments:
- cotangent: bfloat16 [1280, 2048], P('sp'), may hold values from -8 to 8
- saved_input: bfloat16 [1280, 2048], P('sp'), may hold values from -200 to 200
- routes: int32 [1280, 2], P('sp'), may hold values from 0 to 7, all different within a row; in each aligned block of 160 rows (0 to 159, 160 to 319, ...) at most 80 rows name the same one
- route_weight: float32 [1280, 2], P('sp'), may hold values from 0.2 to 1.5
- gate_proj: bfloat16 [8, 2048, 1024], P('sp', None, 'tp'), may hold values from -0.125 to 0.125
- up_proj: bfloat16 [8, 2048, 1024], P('sp', None, 'tp'), may hold values from -0.125 to 0.125
- down_proj: bfloat16 [8, 1024, 2048], P('sp', 'tp'), may hold values from -0.1875 to 0.1875
- out_proj: bfloat16 [2048, 1024], P(None, 'tp'), may hold values from -0.1875 to 0.1875
- conv_input: bfloat16 [1280, 1024], P('sp', 'tp'), may hold values from -6 to 6
- gate_branch: bfloat16 [1280, 1024], P('sp', 'tp'), may hold values from -6 to 6
- conv_taps: bfloat16 [4, 1024], P(None, 'tp'), may hold values from -3 to 3
- recur_map: bfloat16 [2, 16, 64, 64], P(None, 'tp'), may hold values from -0.75 to 0.75
- input_map: bfloat16 [2, 16, 64, 64], P(None, 'tp'), may hold values from -0.75 to 0.75
- decay_param: float32 [2, 1024], P(None, 'tp'), may hold values from 4 to 30
- decay_shift: float32 [2, 1280, 1024], P(None, 'sp', 'tp'), may hold values from -2 to 0, as said below
Outputs:
- grad_gate_proj: float32 [8, 2048, 1024], P('sp', None, 'tp')
- grad_up_proj: float32 [8, 2048, 1024], P('sp', None, 'tp')
- grad_down_proj: float32 [8, 1024, 2048], P('sp', 'tp')
- grad_out_proj: float32 [2048, 1024], P('sp', 'tp')
- grad_conv_input: bfloat16 [1280, 1024], P('sp', 'tp')
- grad_gate_branch: bfloat16 [1280, 1024], P('sp', 'tp')
Inputs may be any that keep to these rules, and one draw needn't show every extreme that they name: Each row names 2 different experts; among the rows of one device no expert is named by more than 80 rows, and in every draw some device routes exactly 80 rows to some expert. `decay_shift`: together with decay_param, -log_decay stays at or above softplus(-decay_param) for every channel and position.
All inputs are finite; a program needn't handle non-finite values.
Results may differ from a plain program's by a relative error of at most 0.013.
Values may be sent and summed in bfloat16 or wider, within the bound.
A program may use at most 128 MiB of HBM per device.

v0:
```python
import jax
import jax.numpy as jnp
from jax import lax
from jax.sharding import PartitionSpec as P

EPS = 1e-06
DECAY_SCALE = 8.0


def with_halo(block, sides, width):
    for axis, dim in sides:
        count = lax.axis_size(axis)
        forward = [(i, i + 1) for i in range(count - 1)]
        backward = [(target, source) for source, target in forward]
        low = lax.ppermute(
            lax.slice_in_dim(block, block.shape[dim] - width, None, axis=dim), axis, forward
        )
        high = lax.ppermute(lax.slice_in_dim(block, 0, width, axis=dim), axis, backward)
        block = jnp.concatenate([low, block, high], axis=dim)
    return block


def prefix(part, axis, combine, identity, reverse):
    count = lax.axis_size(axis)
    place = lax.axis_index(axis)
    ahead = count - 1 - place if reverse else place
    gathered = jax.tree.map(lambda a: lax.all_gather(a, axis), part)
    state = jax.tree.map(lambda a, e: jnp.zeros_like(a) + jnp.asarray(e, a.dtype), part, identity)

    def one(lap, state):
        source = count - 1 - lap if reverse else lap
        return combine(
            state, jax.tree.map(lambda a: lax.dynamic_index_in_dim(a, source, 0, False), gathered)
        )

    return lax.fori_loop(0, ahead, one, state)


def block_matrix(maps):
    heads = maps.shape[0]
    eye = jnp.eye(heads, dtype=jnp.float32)
    full = jnp.einsum("hij,hg->higj", maps.astype(jnp.float32), eye)
    return full.reshape(heads * maps.shape[1], heads * maps.shape[2])


def gate_terms(conv_out, recur_map, input_map, decay_param, decay_shift):
    recur = jax.nn.sigmoid(
        jnp.dot(conv_out, block_matrix(recur_map), precision=lax.Precision.HIGHEST)
    )
    inputs = jax.nn.sigmoid(
        jnp.dot(conv_out, block_matrix(input_map), precision=lax.Precision.HIGHEST)
    )
    log_decay = -DECAY_SCALE * recur * jax.nn.softplus(-decay_param)[None, :] + decay_shift
    decay = jnp.exp(log_decay)
    drive = jnp.sqrt(-jnp.expm1(2.0 * log_decay)) * (inputs * conv_out)
    return (decay, drive)


def link(earlier, later):
    return (earlier[0] * later[0], later[0] * earlier[1] + later[1])


def link_pairs(earlier, later):
    first = link((earlier[0], earlier[1]), (later[0], later[1]))
    second = link((earlier[2], earlier[3]), (later[2], later[3]))
    return first + second


def sweep(coef, drive, reverse):
    return lax.associative_scan(link, (coef, drive), axis=0, reverse=reverse)


def shards(
    cotangent,
    saved_input,
    routes,
    route_weight,
    gate_proj,
    up_proj,
    down_proj,
    out_proj,
    conv_input,
    gate_branch,
    conv_taps,
    recur_map,
    input_map,
    decay_param,
    decay_shift,
):
    length, width = cotangent.shape
    top = routes.shape[1]
    experts = lax.axis_size("sp") * gate_proj.shape[0]
    slots = 4 * length // lax.axis_size("sp")
    inputs32 = saved_input.astype(jnp.float32)
    inv_rms = lax.rsqrt(jnp.mean(inputs32 * inputs32, axis=1, keepdims=True) + EPS)
    normed = inputs32 * inv_rms
    expert_input = normed.astype(jnp.bfloat16)
    scaled = (route_weight[:, :, None] * cotangent.astype(jnp.float32)[:, None, :]).astype(
        jnp.bfloat16
    )
    scaled = scaled.reshape(length * top, width)
    flat_expert = routes.reshape(-1)
    onehot = (flat_expert[:, None] == jnp.arange(experts, dtype=jnp.int32)[None, :]).astype(
        jnp.int32
    )
    earlier_count = jnp.cumsum(onehot, axis=0) - onehot
    rank = jnp.sum(earlier_count * onehot, axis=1)
    target = flat_expert * slots + rank
    token_of = jnp.arange(length * top, dtype=jnp.int32) // top
    fourth = width // lax.axis_size("tp")
    first_col = lax.axis_index("tp") * fourth
    own_scaled = lax.dynamic_slice_in_dim(scaled, first_col, fourth, 1)
    own_input = lax.dynamic_slice_in_dim(expert_input, first_col, fourth, 1)
    send_scaled = jnp.zeros((experts * slots, fourth), jnp.bfloat16).at[target].set(own_scaled)
    send_input = (
        jnp.zeros((experts * slots, fourth), jnp.bfloat16).at[target].set(own_input[token_of])
    )
    part_scaled, part_input = (
        lax.all_to_all(
            send_scaled.reshape(experts, slots, fourth),
            "sp",
            split_axis=0,
            concat_axis=0,
            tiled=True,
        ),
        lax.all_to_all(
            send_input.reshape(experts, slots, fourth),
            "sp",
            split_axis=0,
            concat_axis=0,
            tiled=True,
        ),
    )
    got_scaled, got_input = (
        lax.all_gather(part_scaled, "tp", axis=2, tiled=True),
        lax.all_gather(part_input, "tp", axis=2, tiled=True),
    )
    rows_scaled = got_scaled.reshape(experts * slots, width)
    rows_input = got_input.reshape(experts * slots, width)
    w_gate = gate_proj[0]
    w_up = up_proj[0]
    w_down = down_proj[0]
    gate_pre = jnp.dot(rows_input, w_gate, preferred_element_type=jnp.float32)
    up_pre = jnp.dot(rows_input, w_up, preferred_element_type=jnp.float32)
    gate_sig = jax.nn.sigmoid(gate_pre)
    gate_act = gate_pre * gate_sig
    hidden = (gate_act * up_pre).astype(jnp.bfloat16)
    hidden_grad = lax.dot_general(
        rows_scaled, w_down, (((1,), (1,)), ((), ())), preferred_element_type=jnp.float32
    )
    gate_grad = (hidden_grad * up_pre * gate_sig * (1.0 + gate_pre * (1.0 - gate_sig))).astype(
        jnp.bfloat16
    )
    up_grad = (hidden_grad * gate_act).astype(jnp.bfloat16)
    grad_down = lax.dot_general(
        hidden, rows_scaled, (((0,), (0,)), ((), ())), preferred_element_type=jnp.float32
    )
    grad_gate = lax.dot_general(
        rows_input, gate_grad, (((0,), (0,)), ((), ())), preferred_element_type=jnp.float32
    )
    grad_up = lax.dot_general(
        rows_input, up_grad, (((0,), (0,)), ((), ())), preferred_element_type=jnp.float32
    )
    partial_rows = lax.dot_general(
        gate_grad, w_gate, (((1,), (1,)), ((), ())), preferred_element_type=jnp.float32
    )
    partial_rows = partial_rows + lax.dot_general(
        up_grad, w_up, (((1,), (1,)), ((), ())), preferred_element_type=jnp.float32
    )
    summed = lax.psum(partial_rows.astype(jnp.bfloat16), "tp")
    back = lax.all_to_all(
        summed.reshape(experts, slots, width), "sp", split_axis=0, concat_axis=0, tiled=True
    )
    routed = back.reshape(experts * slots, width)[target].reshape(length, top, width)
    normed_grad = jnp.sum(routed.astype(jnp.float32), axis=1)
    mixed_grad = cotangent.astype(jnp.float32) + inv_rms * (
        normed_grad - normed * jnp.mean(normed_grad * normed, axis=1, keepdims=True)
    )
    mixed_grad_b = mixed_grad.astype(jnp.bfloat16)
    taps32 = conv_taps.astype(jnp.float32)
    padded = with_halo(conv_input, (("sp", 0),), 2)
    conv_out = jnp.zeros((length, padded.shape[1]), jnp.float32)
    for offset in range(taps32.shape[0]):
        conv_out = conv_out + padded[offset : offset + length].astype(jnp.float32) * taps32[offset]
    (coef_f, drive_f), pull_f = jax.vjp(
        lambda value: gate_terms(value, recur_map[0], input_map[0], decay_param[0], decay_shift[0]),
        conv_out,
    )
    (coef_b, drive_b), pull_b = jax.vjp(
        lambda value: gate_terms(value, recur_map[1], input_map[1], decay_param[1], decay_shift[1]),
        conv_out,
    )
    out_grad = jnp.dot(mixed_grad_b, out_proj, preferred_element_type=jnp.float32)
    activated, pull_gelu = jax.vjp(jax.nn.gelu, gate_branch.astype(jnp.float32))
    carried = out_grad * activated
    cum_f, state_f0 = sweep(coef_f, drive_f, False)
    cum_bf, after_b0 = sweep(coef_b, coef_b * carried, False)
    cum_b, state_b0 = sweep(coef_b, drive_b, True)
    cum_fr, after_f0 = sweep(coef_f, coef_f * carried, True)
    ones = jnp.ones((conv_out.shape[1],), jnp.float32)
    zero_filled = jnp.zeros((conv_out.shape[1],), jnp.float32)
    lower = prefix(
        (cum_f[-1], state_f0[-1], cum_bf[-1], after_b0[-1]),
        "sp",
        link_pairs,
        (ones, zero_filled, ones, zero_filled),
        False,
    )
    upper = prefix(
        (cum_b[0], state_b0[0], cum_fr[0], after_f0[0]),
        "sp",
        link_pairs,
        (ones, zero_filled, ones, zero_filled),
        True,
    )
    state_f = state_f0 + cum_f * lower[1][None, :]
    after_b = after_b0 + cum_bf * lower[3][None, :]
    state_b = state_b0 + cum_b * upper[1][None, :]
    after_f = after_f0 + cum_fr * upper[3][None, :]
    adjoint_f = carried + jnp.concatenate([after_f[1:], upper[3][None, :]], axis=0)
    adjoint_b = carried + jnp.concatenate([lower[3][None, :], after_b[:-1]], axis=0)
    prev_f = jnp.concatenate([lower[1][None, :], state_f[:-1]], axis=0)
    next_b = jnp.concatenate([state_b[1:], upper[1][None, :]], axis=0)
    conv_grad = (
        pull_f((adjoint_f * prev_f, adjoint_f))[0] + pull_b((adjoint_b * next_b, adjoint_b))[0]
    )
    states = state_f + state_b
    mixed_out = (activated * states).astype(jnp.bfloat16)
    branch_grad = pull_gelu(out_grad * states)[0].astype(jnp.bfloat16)
    grad_out = lax.psum_scatter(
        lax.dot_general(
            mixed_grad_b, mixed_out, (((0,), (0,)), ((), ())), preferred_element_type=jnp.float32
        ),
        "sp",
        scatter_dimension=0,
        tiled=True,
    )
    grad_pad = with_halo(conv_grad.astype(jnp.bfloat16), (("sp", 0),), 2).astype(conv_grad.dtype)
    input_grad = jnp.zeros((length, conv_grad.shape[1]), jnp.float32)
    for offset in range(taps32.shape[0]):
        input_grad = input_grad + grad_pad[4 - offset : 4 - offset + length] * taps32[offset]
    return (
        grad_gate[None],
        grad_up[None],
        grad_down[None],
        grad_out,
        input_grad.astype(jnp.bfloat16),
        branch_grad,
    )


def solution(mesh):
    in_specs = (
        P("sp", None),
        P("sp", None),
        P("sp", None),
        P("sp", None),
        P("sp", None, "tp"),
        P("sp", None, "tp"),
        P("sp", "tp", None),
        P(None, "tp"),
        P("sp", "tp"),
        P("sp", "tp"),
        P(None, "tp"),
        P(None, "tp", None, None),
        P(None, "tp", None, None),
        P(None, "tp"),
        P(None, "sp", "tp"),
    )
    out_specs = (
        P("sp", None, "tp"),
        P("sp", None, "tp"),
        P("sp", "tp", None),
        P("sp", "tp"),
        P("sp", "tp"),
        P("sp", "tp"),
    )
    return jax.shard_map(shards, mesh=mesh, in_specs=in_specs, out_specs=out_specs, check_vma=False)
```

profile of v0, /device:TPU:0, one launch (start us, length us, event | category | flops | bytes accessed | tf_op | source)
XLA Modules:
  0.0 605.5 jit_solution(16723660355794471832)
XLA Ops:
  16.5 24.9 %all_to_all.15 = bf16[8,80,512]{2,1,0:T(8,128)(2,1)} all-to-all(bf16[8,80,512]{2,1,0:T(8,128)(2,1)S(1)} %bitcast.163), channel_id=1, replica_groups=mesh['sp'=8,'tp'=4] {'sp'}, dimensions={0} | all-to-all | bytes 1310720 | tf_op jit(solution)/shard_map/all_to_all | solution.py:126
  44.3 4.6 mul.743
  51.7 20.7 %all_to_all.16 = bf16[8,80,512]{2,1,0:T(8,128)(2,1)} all-to-all(bf16[8,80,512]{2,1,0:T(8,128)(2,1)S(1)} %bitcast.162), channel_id=1, replica_groups=mesh['sp'=8,'tp'=4] {'sp'}, dimensions={0} | all-to-all | bytes 1310720 | tf_op jit(solution)/shard_map/all_to_all | solution.py:119
  72.8 3.6 fusion.17
  78.1 18.7 %all-gather.13.cloned.1.call-done = bf16[8,80,2048]{2,1,0:T(8,128)(2,1)} async-done(((bf16[8,80,512]{2,1,0:T(8,128)(2,1)}), bf16[8,80,2048]{2,1,0:T(8,128)(2,1)}) %all-gather.13.cloned.1.call-update) | async-done | bytes 2621456 | tf_op jit(solution)/shard_map/all_gather | solution.py:135
  96.8 3.4 multiply_convert_fusion.1
  103.5 60.0 %all-reduce.115.cloned.1.call-done = bf16[8,80,2048]{2,1,0:T(8,128)(2,1)} async-done(((bf16[8,80,2048]{2,1,0:T(8,128)(2,1)}), bf16[8,80,2048]{2,1,0:T(8,128)(2,1)}) %all-reduce.115.cloned.1.call-update) | async-done | bytes 2621456 | tf_op jit(solution)/shard_map/psum | solution.py:170
  163.6 5.5 all-to-all-start.2
  169.1 3.9 collective-permute-start
  186.0 4.2 collective-permute-done
  197.4 30.9 %all-to-all-done.2 = bf16[8,80,2048]{2,1,0:T(8,128)(2,1)S(1)} async-done(((bf16[8,80,2048]{2,1,0:T(8,128)(2,1)}), bf16[8,80,2048]{2,1,0:T(8,128)(2,1)S(1)}, u32[]{:S(2)}, u32[]{:S(2)}) %all-to-all-start.2) | async-done | bytes 2621472 | tf_op jit(solution)/shard_map/all_to_all | solution.py:171
  231.5 4.1 reshape.184
  235.6 5.0 reduce_sum.41
  332.4 22.5 %all-gather.4 = f32[8,1,256]{2,1,0:T(1,128)S(1)} all-gather(f32[1,1,256]{2,1,0:T(1,128)} %add_bitcast_fusion.4), channel_id=1, replica_groups=mesh['sp'=8,'tp'=4] {'sp'}, dimensions={0}, use_global_device_ids=true | all-gather | bytes 9216 | tf_op jit(solution)/shard_map/all_gather | solution.py:27
  354.9 17.1 %all-gather.5 = f32[8,1,256]{2,1,0:T(1,128)S(1)} all-gather(f32[1,1,256]{2,1,0:T(1,128)} %add_bitcast_fusion.3), channel_id=1, replica_groups=mesh['sp'=8,'tp'=4] {'sp'}, dimensions={0}, use_global_device_ids=true | all-gather | bytes 9216 | tf_op jit(solution)/shard_map/all_gather | solution.py:27
  380.1 17.7 %all-gather.6 = f32[8,1,256]{2,1,0:T(1,128)S(1)} all-gather(f32[1,1,256]{2,1,0:T(1,128)S(1)} %add_bitcast_fusion.2), channel_id=1, replica_groups=mesh['sp'=8,'tp'=4] {'sp'}, dimensions={0}, use_global_device_ids=true | all-gather | bytes 9216 | tf_op jit(solution)/shard_map/all_gather | solution.py:27
  398.6 16.9 %all-gather.7 = f32[8,1,256]{2,1,0:T(1,128)S(1)} all-gather(f32[1,1,256]{2,1,0:T(1,128)S(1)} %add_bitcast_fusion.1), channel_id=1, replica_groups=mesh['sp'=8,'tp'=4] {'sp'}, dimensions={0}, use_global_device_ids=true | all-gather | bytes 9216 | tf_op jit(solution)/shard_map/all_gather | solution.py:27
  426.7 17.6 %all-gather = f32[8,1,256]{2,1,0:T(1,128)S(1)} all-gather(f32[1,1,256]{2,1,0:T(1,128)S(1)} %add_bitcast_fusion.8), channel_id=1, replica_groups=mesh['sp'=8,'tp'=4] {'sp'}, dimensions={0}, use_global_device_ids=true | all-gather | bytes 9216 | tf_op jit(solution)/shard_map/all_gather | solution.py:27
  446.6 17.0 %all-gather.1 = f32[8,1,256]{2,1,0:T(1,128)S(1)} all-gather(f32[1,1,256]{2,1,0:T(1,128)S(1)} %add_bitcast_fusion.7), channel_id=1, replica_groups=mesh['sp'=8,'tp'=4] {'sp'}, dimensions={0}, use_global_device_ids=true | all-gather | bytes 9216 | tf_op jit(solution)/shard_map/all_gather | solution.py:27
  480.1 17.6 %all-gather.2 = f32[8,1,256]{2,1,0:T(1,128)S(1)} all-gather(f32[1,1,256]{2,1,0:T(1,128)S(1)} %add_bitcast_fusion.6), channel_id=1, replica_groups=mesh['sp'=8,'tp'=4] {'sp'}, dimensions={0}, use_global_device_ids=true | all-gather | bytes 9216 | tf_op jit(solution)/shard_map/all_gather | solution.py:27
  501.7 17.0 %all-gather.3 = f32[8,1,256]{2,1,0:T(1,128)S(1)} all-gather(f32[1,1,256]{2,1,0:T(1,128)S(1)} %add_bitcast_fusion.5), channel_id=1, replica_groups=mesh['sp'=8,'tp'=4] {'sp'}, dimensions={0}, use_global_device_ids=true | all-gather | bytes 9216 | tf_op jit(solution)/shard_map/all_gather | solution.py:27
  522.5 4.2 convolution_bitcast_fusion.2
  537.4 5.5 collective-permute-start.2
  546.1 52.5 %reduce-scatter.2.cloned.1.call-done = f32[256,256]{1,0:T(8,128)} async-done(((f32[2048,256]{1,0:T(8,128)}), f32[256,256]{1,0:T(8,128)}) %reduce-scatter.2.cloned.1.call-update) | async-done | bytes 262160 | tf_op jit(solution)/shard_map/reduce_scatter | solution.py:230
  (719 shorter events, 194.2 us)
Async XLA Ops:
  7.2 65.6 %copy-start = (bf16[1,2048,256]{2,1,0:T(8,128)(2,1)S(1)}, bf16[1,2048,256]{2,1,0:T(8,128)(2,1)}, u32[]{:S(2)}) copy-start(bf16[1,2048,256]{2,1,0:T(8,128)(2,1)} %param.23) | copy-start | bytes 3145732
  7.2 65.6 %all-gather.11.cloned.1.call-start = ((), (), s32[]{:S(2)}) async-start(), calls=%async_computation.4 | async-start | bytes 3276800 | tf_op jit(solution)/shard_map/all_gather | solution.py:136
  41.4 55.4 %all-gather.13.cloned.1.call-start = ((), (), s32[]{:S(2)}) async-start(), calls=%async_computation.5 | async-start | bytes 3276800 | tf_op jit(solution)/shard_map/all_gather | solution.py:135
  72.5 91.1 %all-reduce.115.cloned.1.call-start = ((), (), s32[]{:S(2)}) async-start(), calls=%async_computation.6 | async-start | bytes 5242880 | tf_op jit(solution)/shard_map/psum | solution.py:170
  103.5 65.6 %copy-start.38 = (bf16[160,256]{1,0:T(8,128)(2,1)S(1)}, bf16[160,256]{1,0:T(8,128)(2,1)}, u32[]{:S(2)}) copy-start(bf16[160,256]{1,0:T(8,128)(2,1)} %param.27) | copy-start | bytes 245764
  103.5 70.9 %copy-start.61 = (f32[2,256]{1,0:T(2,128)S(1)}, f32[2,256]{1,0:T(2,128)}, u32[]{:S(2)}) copy-start(f32[2,256]{1,0:T(2,128)} %param.32) | copy-start | bytes 6148
  103.5 71.5 %copy-start.53 = (bf16[4,256]{1,0:T(4,128)(2,1)S(1)}, bf16[4,256]{1,0:T(4,128)(2,1)}, u32[]{:S(2)}) copy-start(bf16[4,256]{1,0:T(4,128)(2,1)} %param.29) | copy-start | bytes 6148
  163.6 64.7 %all-to-all-start.2 = ((bf16[8,80,2048]{2,1,0:T(8,128)(2,1)}), bf16[8,80,2048]{2,1,0:T(8,128)(2,1)S(1)}, u32[]{:S(2)}, u32[]{:S(2)}) async-start(bf16[8,80,2048]{2,1,0:T(8,128)(2,1)} %all-reduce.115.cloned.1.call-done), calls=%async_computation.2 | async-start | bytes 5242880 | tf_op jit(solution)/shard_map/all_to_all | solution.py:171
  169.1 429.5 %reduce-scatter.2.cloned.1.call-start = ((), (), s32[]{:S(2)}) async-start(), calls=%async_computation.7 | async-start | bytes 2359296 | tf_op jit(solution)/shard_map/reduce_scatter | solution.py:230
  169.1 21.1 %collective-permute-start = (bf16[2,256]{1,0:T(2,128)(2,1)S(1)}, bf16[2,256]{1,0:T(2,128)(2,1)S(1)}, u32[]{:S(2)}, u32[]{:S(2)}) collective-permute-start(bf16[2,256]{1,0:T(2,128)(2,1)S(1)} %get-tuple-element.334), channel_id=1, source_target_pairs={{0,4},{4,8},{8,12},{12,16},{16,20},{20,24},{24,28},{1,5},{5,9},{9,... | collective-permute-start | bytes 3080 | tf_op jit(solution)/shard_map/ppermute | solution.py:15
  173.0 17.2 %collective-permute-start.1 = (bf16[2,256]{1,0:T(2,128)(2,1)S(1)}, bf16[2,256]{1,0:T(2,128)(2,1)S(1)}, u32[]{:S(2)}, u32[]{:S(2)}) collective-permute-start(bf16[2,256]{1,0:T(2,128)(2,1)S(1)} %get-tuple-element.333), channel_id=1, source_target_pairs={{4,0},{8,4},{12,8},{16,12},{20,16},{24,20},{28,24},{5,1},{9,5},{13... | collective-permute-start | bytes 3080 | tf_op jit(solution)/shard_map/ppermute | solution.py:18
  297.5 74.5 %copy-start.29 = (f32[79,256]{1,0:T(8,128)S(1)}, f32[79,256]{1,0:T(8,128)}, u32[]{:S(2)}) copy-start(f32[79,256]{1,0:T(8,128)} %slice.1206) | copy-start | bytes 242692
  308.5 70.4 %copy-start.36 = (f32[19,256]{1,0:T(8,128)S(1)}, f32[19,256]{1,0:T(8,128)}, u32[]{:S(2)}) copy-start(f32[19,256]{1,0:T(8,128)} %slice.1202) | copy-start | bytes 58372
  308.5 70.4 %copy-start.37 = (f32[19,256]{1,0:T(8,128)S(1)}, f32[19,256]{1,0:T(8,128)}, u32[]{:S(2)}) copy-start(f32[19,256]{1,0:T(8,128)} %slice.1167) | copy-start | bytes 58372
  313.8 65.8 %copy-start.57 = (f32[1,256]{1,0:T(1,128)S(1)}, f32[1,256]{1,0:T(1,128)}, u32[]{:S(2)}) copy-start(f32[1,256]{1,0:T(1,128)} %slice.1353) | copy-start | bytes 3076
  313.9 65.8 %copy-start.32 = (f32[39,256]{1,0:T(8,128)S(1)}, f32[39,256]{1,0:T(8,128)}, u32[]{:S(2)}) copy-start(f32[39,256]{1,0:T(8,128)} %slice.1204) | copy-start | bytes 119812
  313.9 65.8 %copy-start.33 = (f32[39,256]{1,0:T(8,128)S(1)}, f32[39,256]{1,0:T(8,128)}, u32[]{:S(2)}) copy-start(f32[39,256]{1,0:T(8,128)} %slice.1169) | copy-start | bytes 119812
  313.9 65.8 %copy-start.60 = (f32[1,256]{1,0:T(1,128)S(1)}, f32[1,256]{1,0:T(1,128)}, u32[]{:S(2)}) copy-start(f32[1,256]{1,0:T(1,128)} %slice.1352) | copy-start | bytes 3076
  315.3 64.5 %copy-start.59 = (f32[1,256]{1,0:T(1,128)S(1)}, f32[1,256]{1,0:T(1,128)}, u32[]{:S(2)}) copy-start(f32[1,256]{1,0:T(1,128)} %slice.1372) | copy-start | bytes 3076
  328.6 51.4 %copy-start.56 = (f32[1,256]{1,0:T(1,128)S(1)}, f32[1,256]{1,0:T(1,128)}, u32[]{:S(2)}) copy-start(f32[1,256]{1,0:T(1,128)} %get-tuple-element.310) | copy-start | bytes 3076
  398.6 47.3 %copy-start.15 = (f32[160,256]{1,0:T(8,128)}, f32[160,256]{1,0:T(8,128)S(1)}, u32[]{:S(2)}) copy-start(f32[160,256]{1,0:T(8,128)S(1)} %pad.459) | copy-start | bytes 491524
  536.1 9.2 %collective-permute-start.3 = (bf16[2,256]{1,0:T(2,128)(2,1)S(1)}, bf16[2,256]{1,0:T(2,128)(2,1)S(1)}, u32[]{:S(2)}, u32[]{:S(2)}) collective-permute-start(bf16[2,256]{1,0:T(2,128)(2,1)S(1)} %get-tuple-element.316), channel_id=1, source_target_pairs={{4,0},{8,4},{12,8},{16,12},{20,16},{24,20},{28,24},{5,1},{9,5},{13... | collective-permute-start | bytes 3080 | tf_op jit(solution)/shard_map/ppermute | solution.py:18
  537.4 61.1 %copy-start.1 = (bf16[1,2048,256]{2,1,0:T(8,128)(2,1)S(1)}, bf16[1,2048,256]{2,1,0:T(8,128)(2,1)}, u32[]{:S(2)}) copy-start(bf16[1,2048,256]{2,1,0:T(8,128)(2,1)} %param.23) | copy-start | bytes 3145732
  537.4 7.8 %collective-permute-start.2 = (bf16[2,256]{1,0:T(2,128)(2,1)S(1)}, bf16[2,256]{1,0:T(2,128)(2,1)S(1)}, u32[]{:S(2)}, u32[]{:S(2)}) collective-permute-start(bf16[2,256]{1,0:T(2,128)(2,1)S(1)} %get-tuple-element.315), channel_id=1, source_target_pairs={{0,4},{4,8},{8,12},{12,16},{16,20},{20,24},{24,28},{1,5},{5,9},{9,... | collective-permute-start | bytes 3080 | tf_op jit(solution)/shard_map/ppermute | solution.py:15
  (55 other events, 742.5 us)
Sparse Core Ops, SparseCore 0:
  41.6 24.1 all-gather.10
  72.6 24.1 all-gather.12
  103.6 59.8 all-reduce.114
  522.6 75.9 reduce-scatter.1
where the time goes:
time: 616 us; the launch traced here: 606 us
  blocking collectives  189 us (31%)
  waiting for transfers between devices  166 us (27%)
  local copies, waits for them, and re-layouts  118 us (19%)
  other arithmetic  64.7 us (11%)
  matrix products  32.2 us (5%)
  starting transfers between devices  17.8 us (3%)
  between operations  16.8 us (3%)
    all_gather x8, blocking collectives, prefix(): gathered = jax.tree.map(lambda a: lax.all_gather(a, axis), part)  143 us
    slice x198, local copies, waits for them, and re-layouts, sweep(): return lax.associative_scan(link, (coef, drive), axis=0, reverse=reverse)  76.2 us
    psum x1, waiting for transfers between devices, shards(): summed = lax.psum(partial_rows.astype(jnp.bfloat16), 'tp')  60 us
    reduce_scatter x1, waiting for transfers between devices, shards(): lax.psum_scatter(lax.dot_general(mixed_grad_b, mixed_out, (((0,), (0,)),...  52.5 us
    all_to_all x1, waiting for transfers between devices, shards(): lax.all_to_all(summed.reshape(experts, slots, width), 'sp', split_axis=0,...  30.9 us
    all_to_all x1, blocking collectives, shards(): lax.all_to_all(send_input.reshape(experts, slots, fourth), 'sp', split_ax...  24.9 us
    concatenate x48, other arithmetic, sweep(): return lax.associative_scan(link, (coef, drive), axis=0, reverse=reverse)  20.9 us
    all_to_all x1, blocking collectives, shards(): lax.all_to_all(send_scaled.reshape(experts, slots, fourth), 'sp', split_a...  20.7 us
  transfers between devices with their start and end apart: 9, of which 5 were waited for; matrix products, arithmetic and copies ran while one was open for 8% of the time, Pallas kernels for 0%

commit v1 on v0

v1 whole, which is shorter than its diff:
```python
import functools
import jax
import jax.numpy as jnp
from jax import lax
from jax.experimental import pallas as pl
from jax.experimental.pallas import tpu as pltpu
from jax.sharding import PartitionSpec as P

EPS = 1e-06
DECAY_SCALE = 8.0
ROW_TILE = 16
GELU_K = 0.7978845608028654
GELU_C = 0.044715
VM = pl.BlockSpec(memory_space=pltpu.VMEM)
BF = jnp.bfloat16
F32 = jnp.float32


def local_call(kernel, args, outs, cost=10_000_000):
    return pl.pallas_call(
        kernel,
        out_shape=outs,
        in_specs=[VM] * len(args),
        out_specs=jax.tree.map(lambda _: VM, outs),
        compiler_params=pltpu.CompilerParams(vmem_limit_bytes=56 * 2**20),
        cost_estimate=pl.CostEstimate(flops=cost, bytes_accessed=4_000_000, transcendentals=0),
    )(*args)


def prepare_kernel(slots, cot_ref, x_ref, routes_ref, weight_ref, sends_ref, sendi_ref, pick_ref):
    length, width = cot_ref.shape
    experts = sends_ref.shape[0]
    fourth = sends_ref.shape[2]
    tp = lax.axis_index("tp")
    cols = pl.ds(pl.multiple_of(tp * fourth, 128), fourth)
    x = x_ref[...].astype(F32)
    inv = lax.rsqrt(jnp.mean(x * x, axis=1, keepdims=True) + EPS)
    mine = (x_ref[:, cols].astype(F32) * inv).astype(BF)
    routes = routes_ref[...]
    weight = weight_ref[...]
    which = lax.broadcasted_iota(jnp.int32, (experts, length), 0)
    first = which == routes[0:1]
    second = which == routes[1:2]
    named = (first | second).astype(F32).astype(BF)
    earlier = lax.broadcasted_iota(jnp.int32, (length, length), 0) < lax.broadcasted_iota(
        jnp.int32, (length, length), 1
    )
    rank = jnp.dot(named, earlier.astype(F32).astype(BF), preferred_element_type=F32)
    place = which * slots + rank.astype(jnp.int32)
    target0 = jnp.sum(jnp.where(first, place, 0).astype(F32), axis=0, keepdims=True).astype(jnp.int32)
    target1 = jnp.sum(jnp.where(second, place, 0).astype(F32), axis=0, keepdims=True).astype(jnp.int32)
    slot = lax.broadcasted_iota(jnp.int32, (experts * slots, length), 0)
    hit0 = slot == target0
    hit1 = slot == target1
    pick = (hit0 | hit1).astype(F32).astype(BF)
    pick_ref[...] = pick
    share = jnp.where(hit0, weight[0:1], 0.0) + jnp.where(hit1, weight[1:2], 0.0)
    share = jnp.sum(share, axis=1, keepdims=True)
    got = jnp.dot(pick, mine, preferred_element_type=F32).astype(BF)
    sendi_ref[...] = got.reshape(experts, slots, fourth)
    cot = jnp.dot(pick, cot_ref[:, cols], preferred_element_type=F32)
    sends_ref[...] = (cot * share).astype(BF).reshape(experts, slots, fourth)


def neighbours():
    tp = lax.axis_index("tp")
    side = tp // 2
    core = tp % 2
    return tp, side * 2 + (1 - core), (1 - side) * 2 + core, (1 - side) * 2 + (1 - core)


def greet(n, with_sp=True, with_tp=True):
    sp = lax.axis_index("sp")
    tp, partner, across, _ = neighbours()
    barrier = pltpu.get_barrier_semaphore()
    count = 0
    if with_sp:
        for d in range(1, n):
            pl.semaphore_signal(
                barrier, inc=1, device_id=((sp + d) % n, tp), device_id_type=pl.DeviceIdType.MESH
            )
        count += n - 1
    if with_tp:
        for other in (partner, across):
            pl.semaphore_signal(
                barrier, inc=1, device_id=(sp, other), device_id_type=pl.DeviceIdType.MESH
            )
        count += 2
    pl.semaphore_wait(barrier, count)


def remote(src, dst, sems, index, device):
    return pltpu.make_async_remote_copy(
        src_ref=src,
        dst_ref=dst,
        send_sem=sems.at[(0,) + index],
        recv_sem=sems.at[(1,) + index],
        device_id=device,
        device_id_type=pl.DeviceIdType.MESH,
    )


def dispatch_kernel(n, sends_ref, sendi_ref, outs_ref, outi_ref, hop, pair, cross, fwd, own):
    fourth = sends_ref.shape[2]
    sp = lax.axis_index("sp")
    tp, partner, across, _ = neighbours()

    def cols(q):
        return pl.ds(pl.multiple_of(q * fourth, 128), fourth)

    mine, theirs = cols(tp), cols(across)
    arrays = ((sends_ref, outs_ref), (sendi_ref, outi_ref))
    greet(n)
    hops = {}
    pending = []
    for a, (src, dst) in enumerate(arrays):
        local = pltpu.make_async_copy(src.at[sp], dst.at[sp, :, mine], own.at[a])
        local.start()
        hops[a, 0] = local
    for d in range(1, n):
        peer = (sp + d) % n
        for a, (src, dst) in enumerate(arrays):
            copy = remote(src.at[peer], dst.at[sp, :, mine], hop, (a, d), (peer, tp))
            copy.start()
            hops[a, d] = copy

    def step_in(a, d):
        dst = arrays[a][1]
        source = (sp + n - d) % n
        if d == 0:
            hops[a, d].wait()
        else:
            hops[a, d].wait_recv()
        block = dst.at[source, :, mine]
        over = remote(block, block, cross, (a, d), (sp, across))
        over.start()
        near = remote(block, block, pair, (a, d), (sp, partner))
        near.start()
        pending.append(near)
        return over

    def step_on(a, d, over):
        dst = arrays[a][1]
        source = (sp + n - d) % n
        over.wait_recv()
        block = dst.at[source, :, theirs]
        copy = remote(block, block, fwd, (a, d), (sp, partner))
        copy.start()
        pending.append(copy)

    order = [(a, d) for d in range(n) for a in range(2)]
    overs = []
    lag = 2
    for i, (a, d) in enumerate(order):
        overs.append(step_in(a, d))
        if i >= lag:
            step_on(*order[i - lag], overs[i - lag])
    for i in range(max(len(order) - lag, 0), len(order)):
        step_on(*order[i], overs[i])
    for copy in pending:
        copy.wait()
    for over in overs:
        over.wait_send()
    for d in range(1, n):
        for a in range(2):
            hops[a, d].wait_send()


def dispatch(sends, sendi, n, n_tp):
    experts, slots, fourth = sends.shape
    full = jax.ShapeDtypeStruct((experts, slots, fourth * n_tp), BF)
    dma = pltpu.SemaphoreType.DMA
    return pl.pallas_call(
        functools.partial(dispatch_kernel, n),
        out_shape=(full, full),
        in_specs=[VM, VM],
        out_specs=(VM, VM),
        scratch_shapes=[dma((2, 2, n))] * 4 + [dma((2,))],
        compiler_params=pltpu.CompilerParams(
            collective_id=1, has_side_effects=True, vmem_limit_bytes=40 * 2**20
        ),
        cost_estimate=pl.CostEstimate(flops=0, bytes_accessed=100_000_000, transcendentals=0),
    )(sends, sendi)


def return_kernel(
    n, part_ref, pick_ref, out_ref, got1, got2, mid, fin, back, s_pair, s_cross, s_hop, s_tail
):
    fourth = got2.shape[2]
    slots = got2.shape[1]
    sp = lax.axis_index("sp")
    tp, partner, across, diagonal = neighbours()

    def cols(q):
        return pl.ds(pl.multiple_of(q * fourth, 128), fourth)

    greet(n)
    order = list(range(1, n)) + [0]
    pairs, crosses, hops = {}, {}, {}
    for d in order:
        j = (sp + d) % n
        for a, q in enumerate((diagonal, partner)):
            copy = remote(
                part_ref.at[j, :, cols(q)], got1.at[a, j], s_pair, (a, d), (sp, partner)
            )
            copy.start()
            pairs[a, d] = copy

    def stage_b(d):
        j = (sp + d) % n
        pairs[0, d].wait_recv()
        total = part_ref[j, :, cols(across)].astype(F32) + got1[0, j].astype(F32)
        mid[j] = total.astype(BF)
        copy = remote(mid.at[j], got2.at[j], s_cross, (d,), (sp, across))
        copy.start()
        crosses[d] = copy

    def stage_c(d):
        j = (sp + d) % n
        pairs[1, d].wait_recv()
        crosses[d].wait_recv()
        total = part_ref[j, :, cols(tp)].astype(F32) + got1[1, j].astype(F32)
        total = (total + got2[j].astype(F32)).astype(BF)
        if d == 0:
            back[sp] = total
        else:
            fin[j] = total
            copy = remote(fin.at[j], back.at[sp], s_hop, (d,), (j, tp))
            copy.start()
            hops[d] = copy

    lag = 2
    for i, d in enumerate(order):
        stage_b(d)
        if i >= lag:
            stage_c(order[i - lag])
    for d in order[max(n - lag, 0):]:
        stage_c(d)
    for d in range(1, n):
        hops[d].wait_recv()
    rows = back[...].reshape(n * slots, fourth)
    grad = lax.dot_general(
        pick_ref[...], rows, (((0,), (0,)), ((), ())), preferred_element_type=F32
    )
    out_ref[:, cols(tp)] = grad.astype(BF)
    own = out_ref.at[:, cols(tp)]
    over = remote(own, own, s_tail, (0,), (sp, across))
    near = remote(own, own, s_tail, (1,), (sp, partner))
    over.start()
    near.start()
    over.wait_recv()
    other = out_ref.at[:, cols(across)]
    last = remote(other, other, s_tail, (2,), (sp, partner))
    last.start()
    for d in range(n):
        for a in range(2):
            pairs[a, d].wait_send()
        crosses[d].wait_send()
        if d:
            hops[d].wait_send()
    near.wait()
    over.wait_send()
    last.wait()


def send_back(part, pick, n, n_tp):
    _, slots, width = part.shape
    fourth = width // n_tp
    dma = pltpu.SemaphoreType.DMA
    block = (n, slots, fourth)
    return pl.pallas_call(
        functools.partial(return_kernel, n),
        out_shape=jax.ShapeDtypeStruct((pick.shape[1], width), BF),
        in_specs=[VM, VM],
        out_specs=VM,
        scratch_shapes=[pltpu.VMEM((2,) + block, BF)]
        + [pltpu.VMEM(block, BF)] * 4
        + [dma((2, 2, n)), dma((2, n)), dma((2, n)), dma((2, 3))],
        compiler_params=pltpu.CompilerParams(
            collective_id=2, has_side_effects=True, vmem_limit_bytes=40 * 2**20
        ),
        cost_estimate=pl.CostEstimate(flops=0, bytes_accessed=100_000_000, transcendentals=0),
    )(part, pick)


def exchange_kernel(n, same, src_ref, dst_ref, sems, own):
    sp = lax.axis_index("sp")
    tp = lax.axis_index("tp")

    def piece(i):
        return src_ref if same else src_ref.at[i]

    greet(n, with_tp=False)
    local = pltpu.make_async_copy(piece(sp), dst_ref.at[sp], own.at[0])
    local.start()
    copies = []
    for d in range(1, n):
        peer = (sp + d) % n
        copy = remote(piece(peer), dst_ref.at[sp], sems, (d,), (peer, tp))
        copy.start()
        copies.append(copy)
    local.wait()
    for copy in copies:
        copy.wait()


def exchange(x, n, same, cid):
    shape = (n,) + x.shape if same else x.shape
    dma = pltpu.SemaphoreType.DMA
    return pl.pallas_call(
        functools.partial(exchange_kernel, n, same),
        out_shape=jax.ShapeDtypeStruct(shape, x.dtype),
        in_specs=[VM],
        out_specs=VM,
        scratch_shapes=[dma((2, n)), dma((1,))],
        compiler_params=pltpu.CompilerParams(
            collective_id=cid, has_side_effects=True, vmem_limit_bytes=24 * 2**20
        ),
        cost_estimate=pl.CostEstimate(flops=0, bytes_accessed=20_000_000, transcendentals=0),
    )(x)


def split_dot(x, w, dims):
    high = x.astype(BF)
    rest = x - high.astype(F32)
    middle = rest.astype(BF)
    low = (rest - middle.astype(F32)).astype(BF)
    total = lax.dot_general(low, w, dims, preferred_element_type=F32)
    total = total + lax.dot_general(middle, w, dims, preferred_element_type=F32)
    return total + lax.dot_general(high, w, dims, preferred_element_type=F32)


def minus_expm1(y):
    series = 1.0 + y * (1.0 / 8.0)
    for k in (7.0, 6.0, 5.0, 4.0, 3.0, 2.0):
        series = 1.0 + y * (1.0 / k) * series
    return jnp.where(y > -0.25, -y * series, 1.0 - jnp.exp(y))


def shifted(x, by, edge):
    length = x.shape[0]
    row = lax.broadcasted_iota(jnp.int32, x.shape, 0)
    moved = pltpu.roll(x, by % length, 0)
    return jnp.where(row == (0 if by > 0 else length - 1), edge, moved)


def run_scans(length, jobs):
    width = jobs[0][1].shape[1]
    groups = length // 8

    def body(g, carry):
        out = []
        for (reverse, a_ref, b_ref, to_ref), state in zip(jobs, carry):
            base = pl.multiple_of((groups - 1 - g if reverse else g) * 8, 8)
            a = a_ref[pl.ds(base, 8), :]
            b = None if b_ref is None else b_ref[pl.ds(base, 8), :]
            rows = [None] * 8
            for k in reversed(range(8)) if reverse else range(8):
                state = a[k : k + 1] * state
                if b is not None:
                    state = state + b[k : k + 1]
                rows[k] = state
            to_ref[pl.ds(base, 8), :] = jnp.concatenate(rows, axis=0)
            out.append(state)
        return tuple(out)

    start = tuple(
        jnp.full((1, width), 1.0 if b_ref is None else 0.0, F32) for _, _, b_ref, _ in jobs
    )
    return lax.fori_loop(0, groups, body, start)


def pre_kernel(
    x_ref, low_ref, high_ref, taps_ref, maps_ref, plus_ref, shift_ref,
    conv_ref, gates_ref, decay_ref, root_ref, state_ref, cum_ref, after_ref, tot_ref, drive_ref,
):
    length, width = x_ref.shape
    taps = taps_ref[...].astype(F32)
    low = low_ref[...].astype(F32)
    high = high_ref[...].astype(F32)
    x = x_ref[...].astype(F32)
    back1 = shifted(x, 1, low[1:2])
    back2 = shifted(back1, 1, low[0:1])
    conv = back2 * taps[0:1] + back1 * taps[1:2] + x * taps[2:3]
    conv = conv + shifted(x, -1, high[0:1]) * taps[3:4]
    conv_ref[...] = conv
    gates = jax.nn.sigmoid(split_dot(conv, maps_ref[...], (((1,), (0,)), ((), ()))))
    gates_ref[...] = gates
    for d in range(2):
        recur = gates[:, 2 * d * width : (2 * d + 1) * width]
        inputs = gates[:, (2 * d + 1) * width : (2 * d + 2) * width]
        log_decay = -DECAY_SCALE * recur * plus_ref[d : d + 1, :] + shift_ref[d]
        root = jnp.sqrt(minus_expm1(2.0 * log_decay))
        decay_ref[d] = jnp.exp(log_decay)
        root_ref[d] = root
        drive_ref[d] = root * (inputs * conv)
    a_f, a_b = decay_ref.at[0], decay_ref.at[1]
    ends = run_scans(
        length,
        (
            (False, a_f, drive_ref.at[0], state_ref.at[0]),
            (True, a_b, drive_ref.at[1], state_ref.at[1]),
            (False, a_f, None, cum_ref.at[0]),
            (True, a_b, None, cum_ref.at[1]),
            (True, a_f, None, after_ref.at[0]),
            (False, a_b, None, after_ref.at[1]),
        ),
    )
    tot_ref[0:1, :] = ends[2]
    tot_ref[1:2, :] = ends[0]
    tot_ref[2:3, :] = ends[3]
    tot_ref[3:4, :] = ends[1]
    tot_ref[4:8, :] = jnp.zeros((4, width), F32)


def gelu_parts(x):
    t = jnp.tanh(GELU_K * (x + GELU_C * x * x * x))
    value = 0.5 * x * (1.0 + t)
    slope = 0.5 * (1.0 + t) + 0.5 * x * (1.0 - t * t) * GELU_K * (1.0 + 3.0 * GELU_C * x * x)
    return value, slope


def middle_kernel(
    ng_ref, cot_ref, x_ref, proj_ref, branch_ref, decay_ref, tot_ref,
    mixed_ref, out_grad_ref, carried_ref, after_ref, tot2_ref, drive_ref,
):
    length = ng_ref.shape[0]
    x = x_ref[...].astype(F32)
    inv = lax.rsqrt(jnp.mean(x * x, axis=1, keepdims=True) + EPS)
    normed = x * inv
    ng = ng_ref[...].astype(F32)
    dot = jnp.mean(ng * normed, axis=1, keepdims=True)
    mixed = (cot_ref[...].astype(F32) + inv * (ng - normed * dot)).astype(BF)
    mixed_ref[...] = mixed
    out_grad = jnp.dot(mixed, proj_ref[...], preferred_element_type=F32)
    out_grad_ref[...] = out_grad
    value, _ = gelu_parts(branch_ref[...].astype(F32))
    carried = out_grad * value
    carried_ref[...] = carried
    drive_ref[...] = decay_ref[...] * carried[None]
    ends = run_scans(
        length,
        (
            (True, decay_ref.at[0], drive_ref.at[0], after_ref.at[0]),
            (False, decay_ref.at[1], drive_ref.at[1], after_ref.at[1]),
        ),
    )
    tot2_ref[0:4, :] = tot_ref[0:4, :]
    tot2_ref[4:5, :] = ends[1]
    tot2_ref[5:6, :] = ends[0]
    tot2_ref[6:8, :] = jnp.zeros((2, tot_ref.shape[1]), F32)


def last_kernel(
    n, all_ref, conv_ref, gates_ref, decay_ref, root_ref, state_ref, cum_ref, ones_ref,
    after_ref, carried_ref, out_grad_ref, branch_ref, maps_ref, plus_ref,
    conv_grad_ref, branch_grad_ref, mixed_out_ref, packed_ref,
):
    length, width = conv_ref.shape
    sp = lax.axis_index("sp")
    zero = jnp.zeros((1, width), F32)

    def lower(k, carry):
        t = all_ref[k]
        return (t[0:1] * carry[0] + t[1:2], t[2:3] * carry[1] + t[4:5])

    def upper(i, carry):
        t = all_ref[n - 1 - i]
        return (t[2:3] * carry[0] + t[3:4], t[0:1] * carry[1] + t[5:6])

    in_f, in_ab = lax.fori_loop(0, sp, lower, (zero, zero))
    in_b, in_af = lax.fori_loop(0, n - 1 - sp, upper, (zero, zero))
    state_f = state_ref[0] + cum_ref[0] * in_f
    state_b = state_ref[1] + cum_ref[1] * in_b
    after_f = after_ref[0] + ones_ref[0] * in_af
    after_b = after_ref[1] + ones_ref[1] * in_ab
    carried = carried_ref[...]
    adjoint = (carried + shifted(after_f, -1, in_af), carried + shifted(after_b, 1, in_ab))
    beside = (shifted(state_f, 1, in_f), shifted(state_b, -1, in_b))
    conv = conv_ref[...]
    total = jnp.zeros((length, width), F32)
    for d in range(2):
        recur = gates_ref[:, 2 * d * width : (2 * d + 1) * width]
        inputs = gates_ref[:, (2 * d + 1) * width : (2 * d + 2) * width]
        decay = decay_ref[d]
        root = root_ref[d]
        g = adjoint[d]
        total = total + g * root * inputs
        g_log = g * beside[d] * decay - g * inputs * conv * (decay * decay) / root
        g_recur = g_log * (-DECAY_SCALE * plus_ref[d : d + 1, :])
        packed_ref[:, 2 * d * width : (2 * d + 1) * width] = g_recur * recur * (1.0 - recur)
        packed_ref[:, (2 * d + 1) * width : (2 * d + 2) * width] = (
            g * root * conv * inputs * (1.0 - inputs)
        )
    total = total + split_dot(packed_ref[...], maps_ref[...], (((1,), (1,)), ((), ())))
    conv_grad_ref[...] = total.astype(BF)
    value, slope = gelu_parts(branch_ref[...].astype(F32))
    states = state_f + state_b
    mixed_out_ref[...] = (value * states).astype(BF)
    branch_grad_ref[...] = (out_grad_ref[...] * states * slope).astype(BF)


def block_matrix(maps):
    heads = maps.shape[0]
    eye = jnp.eye(heads, dtype=maps.dtype)
    full = maps[:, :, None, :] * eye[:, None, :, None]
    return full.reshape(heads * maps.shape[1], heads * maps.shape[2])


def edge_rows(block, n, width):
    forward = [(i, i + 1) for i in range(n - 1)]
    backward = [(i + 1, i) for i in range(n - 1)]
    low = lax.ppermute(block[block.shape[0] - width :], "sp", forward)
    high = lax.ppermute(block[:width], "sp", backward)
    return low, high


def shards(
    cotangent,
    saved_input,
    routes,
    route_weight,
    gate_proj,
    up_proj,
    down_proj,
    out_proj,
    conv_input,
    gate_branch,
    conv_taps,
    recur_map,
    input_map,
    decay_param,
    decay_shift,
):
    length, width = cotangent.shape
    n = lax.axis_size("sp")
    n_tp = lax.axis_size("tp")
    experts = n * gate_proj.shape[0]
    slots = 4 * length // n
    slots = (slots + ROW_TILE - 1) // ROW_TILE * ROW_TILE
    fourth = width // n_tp
    channels = conv_input.shape[1]
    sds = jax.ShapeDtypeStruct

    low, high = edge_rows(conv_input, n, 2)
    sends, sendi, pick = local_call(
        functools.partial(prepare_kernel, slots),
        (cotangent, saved_input, routes.T, route_weight.T),
        (
            sds((experts, slots, fourth), BF),
            sds((experts, slots, fourth), BF),
            sds((experts * slots, length), BF),
        ),
    )
    got_scaled, got_input = dispatch(sends, sendi, n, n_tp)
    rows_scaled = got_scaled.reshape(experts * slots, width)
    rows_input = got_input.reshape(experts * slots, width)
    w_gate = gate_proj[0]
    w_up = up_proj[0]
    w_down = down_proj[0]
    gate_pre = jnp.dot(rows_input, w_gate, preferred_element_type=F32)
    up_pre = jnp.dot(rows_input, w_up, preferred_element_type=F32)
    gate_sig = jax.nn.sigmoid(gate_pre)
    gate_act = gate_pre * gate_sig
    hidden = (gate_act * up_pre).astype(BF)
    hidden_grad = lax.dot_general(
        rows_scaled, w_down, (((1,), (1,)), ((), ())), preferred_element_type=F32
    )
    gate_grad = (hidden_grad * up_pre * gate_sig * (1.0 + gate_pre * (1.0 - gate_sig))).astype(BF)
    up_grad = (hidden_grad * gate_act).astype(BF)
    partial_rows = lax.dot_general(
        gate_grad, w_gate, (((1,), (1,)), ((), ())), preferred_element_type=F32
    )
    partial_rows = partial_rows + lax.dot_general(
        up_grad, w_up, (((1,), (1,)), ((), ())), preferred_element_type=F32
    )
    part = partial_rows.astype(BF).reshape(experts, slots, width)
    normed_grad = send_back(part, pick, n, n_tp)
    rows0 = (((0,), (0,)), ((), ()))
    grad_down = lax.dot_general(hidden, rows_scaled, rows0, preferred_element_type=F32)
    grad_gate = lax.dot_general(rows_input, gate_grad, rows0, preferred_element_type=F32)
    grad_up = lax.dot_general(rows_input, up_grad, rows0, preferred_element_type=F32)

    maps = jnp.concatenate(
        [block_matrix(m[d]) for d in range(2) for m in (recur_map, input_map)], axis=1
    )
    plus = jax.nn.softplus(-decay_param)
    one = sds((length, channels), F32)
    two = sds((2, length, channels), F32)
    eight = sds((8, channels), F32)
    conv, gates, decay, root, state, cum, ones, tot, _ = local_call(
        pre_kernel,
        (conv_input, low, high, conv_taps, maps, plus, decay_shift),
        (one, sds((length, 4 * channels), F32), two, two, two, two, two, eight, two),
    )
    mixed_grad_b, out_grad, carried, after, tot2, _ = local_call(
        middle_kernel,
        (normed_grad, cotangent, saved_input, out_proj, gate_branch, decay, tot),
        (sds((length, width), BF), one, one, two, eight, two),
    )
    everyone = exchange(tot2, n, True, 3)
    conv_grad, branch_grad, mixed_out, _ = local_call(
        functools.partial(last_kernel, n),
        (
            everyone, conv, gates, decay, root, state, cum, ones, after, carried, out_grad,
            gate_branch, maps, plus,
        ),
        (
            sds((length, channels), BF),
            sds((length, channels), BF),
            sds((length, channels), BF),
            sds((length, 4 * channels), F32),
        ),
    )
    grad_low, grad_high = edge_rows(conv_grad, n, 2)
    grad_part = lax.dot_general(mixed_grad_b, mixed_out, rows0, preferred_element_type=F32)
    pieces = exchange(grad_part.astype(BF).reshape(n, width // n, channels), n, False, 4)
    grad_out = jnp.sum(pieces.astype(F32), axis=0)
    taps32 = conv_taps.astype(F32)
    grad_pad = jnp.concatenate([grad_low, conv_grad, grad_high], axis=0).astype(F32)
    input_grad = jnp.zeros((length, channels), F32)
    for offset in range(taps32.shape[0]):
        input_grad = input_grad + grad_pad[4 - offset : 4 - offset + length] * taps32[offset]
    return (
        grad_gate[None],
        grad_up[None],
        grad_down[None],
        grad_out,
        input_grad.astype(BF),
        branch_grad,
    )


def solution(mesh):
    in_specs = (
        P("sp", None),
        P("sp", None),
        P("sp", None),
        P("sp", None),
        P("sp", None, "tp"),
        P("sp", None, "tp"),
        P("sp", "tp", None),
        P(None, "tp"),
        P("sp", "tp"),
        P("sp", "tp"),
        P(None, "tp"),
        P(None, "tp", None, None),
        P(None, "tp", None, None),
        P(None, "tp"),
        P(None, "sp", "tp"),
    )
    out_specs = (
        P("sp", None, "tp"),
        P("sp", None, "tp"),
        P("sp", "tp", None),
        P("sp", "tp"),
        P("sp", "tp"),
        P("sp", "tp"),
    )
    return jax.shard_map(shards, mesh=mesh, in_specs=in_specs, out_specs=out_specs, check_vma=False)
```

time: 616 us -> 173 us (0.28)
  the two profiles are of different devices: /device:TPU:0 before, /device:TPU:16 now
where the time goes in v1:
time: 173 us
  Pallas kernels  128 us (74%)
  matrix products  14.4 us (8%)
  starting transfers between devices  13.9 us (8%)
  local copies, waits for them, and re-layouts  9.5 us (5%)
  waiting for transfers between devices  3.6 us (2%)
  other arithmetic  2.78 us (2%)
    pallas_call x1, Pallas kernels, send_back(): pl.pallas_call(functools.partial(return_kernel, n), out_shape=jax.ShapeDt...  40.2 us
    pallas_call x2, Pallas kernels, exchange(): pl.pallas_call(functools.partial(exchange_kernel, n, same), out_shape=jax...  35.9 us
    pallas_call x1, Pallas kernels, dispatch(): pl.pallas_call(functools.partial(dispatch_kernel, n), out_shape=(full, fu...  35.6 us
    pallas_call x4, Pallas kernels, local_call(): pl.pallas_call(kernel, out_shape=outs, in_specs=[VM] * len(args), out_spe...  16 us
    ppermute x2, starting transfers between devices, edge_rows(): high = lax.ppermute(block[:width], 'sp', backward)  8.6 us
    unnamed x41, local copies, waits for them, and re-layouts  7.8 us
    ppermute x2, starting transfers between devices, edge_rows(): low = lax.ppermute(block[block.shape[0] - width:], 'sp', forward)  5.34 us
    ppermute x2, waiting for transfers between devices, edge_rows(): low = lax.ppermute(block[block.shape[0] - width:], 'sp', forward)  3.59 us
  transfers between devices with their start and end apart: 4, of which 1 were waited for; matrix products, arithmetic and copies ran while one was open for 9% of the time, Pallas kernels for 46%

profile of v1, /device:TPU:16, one launch (start us, length us, event | category | flops | bytes accessed | tf_op | source)
XLA Modules:
  0.0 172.8 jit_solution(10845798235887398941)
XLA Ops:
  1.4 3.4 %collective-permute-start = (bf16[2,256]{1,0:T(2,128)(2,1)S(1)}, bf16[2,256]{1,0:T(2,128)(2,1)S(1)}, u32[]{:S(2)}, u32[]{:S(2)}) collective-permute-start(bf16[2,256]{1,0:T(2,128)(2,1)S(1)} %get-tuple-element.57), channel_id=1, source_target_pairs={{0,4},{4,8},{8,12},{12,16},{16,20},{20,24},{24,28},{1,5},{5,9},{9,... | collective-permute-start | bytes 3080 | tf_op jit(solution)/shard_map/ppermute | solution.py:513
  4.9 3.3 %collective-permute-start.1 = (bf16[2,256]{1,0:T(2,128)(2,1)S(1)}, bf16[2,256]{1,0:T(2,128)(2,1)S(1)}, u32[]{:S(2)}, u32[]{:S(2)}) collective-permute-start(bf16[2,256]{1,0:T(2,128)(2,1)S(1)} %get-tuple-element.56), channel_id=1, source_target_pairs={{4,0},{8,4},{12,8},{16,12},{20,16},{24,20},{28,24},{5,1},{9,5},{13... | collective-permute-start | bytes 3080 | tf_op jit(solution)/shard_map/ppermute | solution.py:514
  8.2 3.2 %shard_map.190 = (bf16[8,80,512]{2,1,0:T(8,128)(2,1)}, bf16[8,80,512]{2,1,0:T(8,128)(2,1)}, bf16[640,160]{1,0:T(8,128)(2,1)}) custom-call(bf16[160,2048]{1,0:T(8,128)(2,1)} %cot_ref.3, bf16[160,2048]{1,0:T(8,128)(2,1)} %x_ref.5, s32[2,160]{1,0:T(2,128)} %bitcast.63, f32[2,160]{1,0:T(2,128)} %bitcast.64), custom_call_target="tpu_custom_call" | custom-call | flops 10000000 | bytes 4000000 | tf_op jit(solution)/shard_map/pallas_call | solution.py:20
  11.3 1.1 copy-done.3
  12.4 1.1 copy-done.4
  13.5 35.6 %shard_map.191 = (bf16[8,80,2048]{2,1,0:T(8,128)(2,1)S(1)}, bf16[8,80,2048]{2,1,0:T(8,128)(2,1)S(1)}) custom-call(bf16[8,80,512]{2,1,0:T(8,128)(2,1)S(1)} %copy-done.3, bf16[8,80,512]{2,1,0:T(8,128)(2,1)S(1)} %copy-done.4), custom_call_target="tpu_custom_call" | custom-call | bytes 100000000 | tf_op jit(solution)/shard_map/pallas_call | solution.py:173
  49.1 0.8 fusion.2
  51.2 2.4 %convolution_bitcast_fusion = f32[1,256,2048]{2,1,0:T(8,128)} fusion(bf16[640,2048]{1,0:T(8,128)(2,1)S(1)} %bitcast.57, f32[640,256]{1,0:T(8,128)S(1)} %fusion.5, f32[640,256]{1,0:T(8,128)S(1)} %fusion.2), kind=kOutput, calls=%fused_computation.1 | convolution fusion | flops 672071680 | bytes 6029312 | tf_op jit(solution)/shard_map/dot_general | solution.py:580
  53.6 1.0 multiply_convert_fusion.1
  54.6 2.3 %convolution_bitcast_fusion.2 = f32[1,2048,256]{2,1,0:T(8,128)} fusion(bf16[640,2048]{1,0:T(8,128)(2,1)S(1)} %bitcast.55, bf16[640,256]{1,0:T(8,128)(2,1)S(1)} %get-tuple-element.49), kind=kOutput, calls=%fused_computation.3 | convolution fusion | flops 671088640 | bytes 5046272 | tf_op jit(solution)/shard_map/dot_general | solution.py:581
  56.9 0.9 fusion
  57.8 2.3 %convolution_bitcast_fusion.1 = f32[1,2048,256]{2,1,0:T(8,128)} fusion(bf16[640,2048]{1,0:T(8,128)(2,1)S(1)} %bitcast.56, bf16[640,256]{1,0:T(8,128)(2,1)S(1)} %get-tuple-element.48), kind=kOutput, calls=%fused_computation.2 | convolution fusion | flops 671088640 | bytes 5046272 | tf_op jit(solution)/shard_map/dot_general | solution.py:582
  60.1 2.4 %add_convert_fusion = bf16[640,2048]{1,0:T(8,128)(2,1)} fusion(f32[640,2048]{1,0:T(8,128)S(1)} %fusion, bf16[640,256]{1,0:T(8,128)(2,1)S(1)} %get-tuple-element.48, bf16[1,2048,256]{2,1,0:T(8,128)(2,1)S(1)} %copy-done.9), kind=kOutput, calls=%fused_computation | convolution fusion | flops 673710080 | bytes 9240576 | tf_op jit(solution)/shard_map/dot_general | solution.py:574
  64.8 1.9 %copy-done.1 = bf16[640,2048]{1,0:T(8,128)(2,1)S(1)} copy-done((bf16[640,2048]{1,0:T(8,128)(2,1)S(1)}, bf16[640,2048]{1,0:T(8,128)(2,1)}, u32[]{:S(2)}) %copy-start.1) | copy-done | bytes 2621464
  66.7 40.2 %shard_map.192.ng_ref = bf16[160,2048]{1,0:T(8,128)(2,1)S(1)} custom-call(bf16[8,80,2048]{2,1,0:T(8,128)(2,1)S(1)} %bitcast.51, bf16[640,160]{1,0:T(8,128)(2,1)S(1)} %copy-done.5), custom_call_target="tpu_custom_call" | custom-call | bytes 100000000 | tf_op jit(solution)/shard_map/pallas_call | solution.py:271
  108.8 4.6 %shard_map.193 = (f32[160,256]{1,0:T(8,128)}, f32[160,1024]{1,0:T(8,128)}, f32[2,160,256]{2,1,0:T(8,128)}, f32[2,160,256]{2,1,0:T(8,128)}, f32[2,160,256]{2,1,0:...) custom-call(bf16[160,256]{1,0:T(8,128)(2,1)} %x_ref.4, ...), custom_call_target="tpu_custom_call" | custom-call | flops 10000000 | bytes 4000000 | tf_op jit(solution)/shard_map/pallas_call | solution.py:20
  113.5 4.5 %shard_map.194 = (bf16[160,2048]{1,0:T(8,128)(2,1)}, f32[160,256]{1,0:T(8,128)}, f32[160,256]{1,0:T(8,128)}, f32[2,160,256]{2,1,0:T(8,128)}, f32[8,256]{1,0:T(8,128)}, /*index=5*/f32[2,160,256]{2,1,0:T(8,128)}) custom-call(bf16[160,2048]{1,0:T(8,128)(2,1)} %copy-done.2, bf16[160,2048]{1,0:T(8,128)(2,1)} %cot_ref.3, bf16[160,2048]{1,0:T(8,128)(2,1)} %x_ref.5, ...), custom_call_target="tpu_custom_call" | custom-call | flops 10000000 | bytes 4000000 | tf_op jit(solution)/shard_map/pallas_call | solution.py:20
  118.7 10.7 %shard_map.195.all_ref = f32[8,8,256]{2,1,0:T(8,128)S(1)} custom-call(f32[8,256]{1,0:T(8,128)S(1)} %copy-done.7), custom_call_target="tpu_custom_call" | custom-call | bytes 20000000 | tf_op jit(solution)/shard_map/pallas_call | solution.py:310
  130.0 3.7 %shard_map.196 = (bf16[160,256]{1,0:T(8,128)(2,1)}, bf16[160,256]{1,0:T(8,128)(2,1)}, bf16[160,256]{1,0:T(8,128)(2,1)}, f32[160,1024]{1,0:T(8,128)}) custom-call(f32[8,8,256]{2,1,0:T(8,128)} %copy-done.6, f32[160,256]{1,0:T(8,128)} %get-tuple-element.36.conv_ref, f32[160,1024]{1,0:T(8,128)} %get-tuple-element.37.gates_ref, ...), custom_call_target="tpu_custom_call" | custom-call | flops 10000000 | bytes 4000000 | tf_op jit(solution)/shard_map/pallas_call | solution.py:20
  133.7 1.4 convolution_convert_fusion
  135.2 25.2 %shard_map.197 = bf16[8,256,256]{2,1,0:T(8,128)(2,1)S(1)} custom-call(bf16[8,256,256]{2,1,0:T(8,128)(2,1)S(1)} %bitcast.52), custom_call_target="tpu_custom_call" | custom-call | bytes 20000000 | tf_op jit(solution)/shard_map/pallas_call | solution.py:310
  160.4 5.3 %collective-permute-start.3 = (bf16[2,256]{1,0:T(2,128)(2,1)S(1)}, bf16[2,256]{1,0:T(2,128)(2,1)S(1)}, u32[]{:S(2)}, u32[]{:S(2)}) collective-permute-start(bf16[2,256]{1,0:T(2,128)(2,1)S(1)} %get-tuple-element.55), channel_id=1, source_target_pairs={{4,0},{8,4},{12,8},{16,12},{20,16},{24,20},{28,24},{5,1},{9,5},{13... | collective-permute-start | bytes 3080 | tf_op jit(solution)/shard_map/ppermute | solution.py:514
  165.7 1.9 %collective-permute-start.2 = (bf16[2,256]{1,0:T(2,128)(2,1)S(1)}, bf16[2,256]{1,0:T(2,128)(2,1)S(1)}, u32[]{:S(2)}, u32[]{:S(2)}) collective-permute-start(bf16[2,256]{1,0:T(2,128)(2,1)S(1)} %get-tuple-element.54), channel_id=1, source_target_pairs={{0,4},{4,8},{8,12},{12,16},{16,20},{20,24},{24,28},{1,5},{5,9},{9,... | collective-permute-start | bytes 3080 | tf_op jit(solution)/shard_map/ppermute | solution.py:513
  168.4 3.6 %collective-permute-done.2 = bf16[2,256]{1,0:T(2,128)(2,1)S(1)} collective-permute-done((bf16[2,256]{1,0:T(2,128)(2,1)S(1)}, bf16[2,256]{1,0:T(2,128)(2,1)S(1)}, u32[]{:S(2)}, u32[]{:S(2)}) %collective-permute-start.2) | collective-permute-done | bytes 1056 | tf_op jit(solution)/shard_map/ppermute | solution.py:513
  (57 shorter events, 9.0 us)
Async XLA Ops:
  0.6 48.5 %copy-start = (bf16[1,2048,256]{2,1,0:T(8,128)(2,1)S(1)}, bf16[1,2048,256]{2,1,0:T(8,128)(2,1)}, u32[]{:S(2)}) copy-start(bf16[1,2048,256]{2,1,0:T(8,128)(2,1)} %param.19) | copy-start | bytes 3145732
  1.4 106.2 %collective-permute-start = (bf16[2,256]{1,0:T(2,128)(2,1)S(1)}, bf16[2,256]{1,0:T(2,128)(2,1)S(1)}, u32[]{:S(2)}, u32[]{:S(2)}) collective-permute-start(bf16[2,256]{1,0:T(2,128)(2,1)S(1)} %get-tuple-element.57), channel_id=1, source_target_pairs={{0,4},{4,8},{8,12},{12,16},{16,20},{20,24},{24,28},{1,5},{5,9},{9,... | collective-permute-start | bytes 3080 | tf_op jit(solution)/shard_map/ppermute | solution.py:513
  4.9 102.8 %collective-permute-start.1 = (bf16[2,256]{1,0:T(2,128)(2,1)S(1)}, bf16[2,256]{1,0:T(2,128)(2,1)S(1)}, u32[]{:S(2)}, u32[]{:S(2)}) collective-permute-start(bf16[2,256]{1,0:T(2,128)(2,1)S(1)} %get-tuple-element.56), channel_id=1, source_target_pairs={{4,0},{8,4},{12,8},{16,12},{20,16},{24,20},{28,24},{5,1},{9,5},{13... | collective-permute-start | bytes 3080 | tf_op jit(solution)/shard_map/ppermute | solution.py:514
  11.3 1.1 copy-start.3
  12.4 1.1 copy-start.4
  49.1 1.2 copy-start.9
  51.2 2.4 %copy-start.18 = (bf16[1,256,2048]{2,1,0:T(8,128)(2,1)S(1)}, bf16[1,256,2048]{2,1,0:T(8,128)(2,1)}, u32[]{:S(2)}) copy-start(bf16[1,256,2048]{2,1,0:T(8,128)(2,1)} %param.21) | copy-start | bytes 3145732
  60.1 2.4 %copy-start.11 = (bf16[2,4,64,64]{3,2,1,0:T(8,128)(2,1)S(1)}, bf16[2,4,64,64]{3,2,1,0:T(8,128)(2,1)}, u32[]{:S(2)}) copy-start(bf16[2,4,64,64]{3,2,1,0:T(8,128)(2,1)} %param.27) | copy-start | bytes 196612
  60.1 2.4 %copy-start.12 = (bf16[2,4,64,64]{3,2,1,0:T(8,128)(2,1)S(1)}, bf16[2,4,64,64]{3,2,1,0:T(8,128)(2,1)}, u32[]{:S(2)}) copy-start(bf16[2,4,64,64]{3,2,1,0:T(8,128)(2,1)} %param.26) | copy-start | bytes 196612
  62.5 1.5 copy-start.15
  62.5 2.1 %copy-start.14 = (bf16[4,256]{1,0:T(4,128)(2,1)S(1)}, bf16[4,256]{1,0:T(4,128)(2,1)}, u32[]{:S(2)}) copy-start(bf16[4,256]{1,0:T(4,128)(2,1)} %taps_ref.1) | copy-start | bytes 6148
  62.5 2.2 %copy-start.5 = (bf16[640,160]{1,0:T(8,128)(2,1)S(1)}, bf16[640,160]{1,0:T(8,128)(2,1)}, u32[]{:S(2)}) copy-start(bf16[640,160]{1,0:T(8,128)(2,1)} %get-tuple-element.31.pick_ref) | copy-start | bytes 614404
  64.7 43.0 %copy-start.8 = (bf16[256,1024]{1,0:T(8,128)(2,1)}, bf16[256,1024]{1,0:T(8,128)(2,1)S(1)}, u32[]{:S(2)}) copy-start(bf16[256,1024]{1,0:T(8,128)(2,1)S(1)} %constant_dynamic-update-slice_fusion.maps_ref) | copy-start | bytes 1572868
  64.7 1.9 %copy-start.1 = (bf16[640,2048]{1,0:T(8,128)(2,1)S(1)}, bf16[640,2048]{1,0:T(8,128)(2,1)}, u32[]{:S(2)}) copy-start(bf16[640,2048]{1,0:T(8,128)(2,1)} %add_convert_fusion) | copy-start | bytes 7864324
  106.8 0.8 copy-start.2
  107.7 0.6 copy-start.16
  108.3 0.6 copy-start.17
  118.0 0.7 copy-start.7
  118.7 15.0 %copy-start.10 = (bf16[160,2048]{1,0:T(8,128)(2,1)S(1)}, bf16[160,2048]{1,0:T(8,128)(2,1)}, u32[]{:S(2)}) copy-start(bf16[160,2048]{1,0:T(8,128)(2,1)} %get-tuple-element.34) | copy-start | bytes 1966084
  129.4 0.6 copy-start.6
  133.7 26.6 %copy-start.13 = (bf16[160,256]{1,0:T(8,128)(2,1)S(1)}, bf16[160,256]{1,0:T(8,128)(2,1)}, u32[]{:S(2)}) copy-start(bf16[160,256]{1,0:T(8,128)(2,1)} %get-tuple-element.46) | copy-start | bytes 245764
  160.4 8.1 %collective-permute-start.3 = (bf16[2,256]{1,0:T(2,128)(2,1)S(1)}, bf16[2,256]{1,0:T(2,128)(2,1)S(1)}, u32[]{:S(2)}, u32[]{:S(2)}) collective-permute-start(bf16[2,256]{1,0:T(2,128)(2,1)S(1)} %get-tuple-element.55), channel_id=1, source_target_pairs={{4,0},{8,4},{12,8},{16,12},{20,16},{24,20},{28,24},{5,1},{9,5},{13... | collective-permute-start | bytes 3080 | tf_op jit(solution)/shard_map/ppermute | solution.py:514
  165.7 6.4 %collective-permute-start.2 = (bf16[2,256]{1,0:T(2,128)(2,1)S(1)}, bf16[2,256]{1,0:T(2,128)(2,1)S(1)}, u32[]{:S(2)}, u32[]{:S(2)}) collective-permute-start(bf16[2,256]{1,0:T(2,128)(2,1)S(1)} %get-tuple-element.54), channel_id=1, source_target_pairs={{0,4},{4,8},{8,12},{12,16},{16,20},{20,24},{24,28},{1,5},{5,9},{9,... | collective-permute-start | bytes 3080 | tf_op jit(solution)/shard_map/ppermute | solution.py:513

commit v2 on v1

--- a/solution.py
+++ b/solution.py
@@ -89,6 +89,43 @@
     pl.semaphore_wait(barrier, count)
 
 
+def partner_at(sp, n, d):
+    if n & (n - 1):
+        return (sp + d) % n
+    bit, peer = 1, sp
+    while bit < n:
+        if d & bit:
+            peer = peer + bit * (1 - 2 * ((sp // bit) % 2))
+        bit *= 2
+    return peer
+
+
+def source_at(sp, n, d):
+    return (sp + n - d) % n if n & (n - 1) else partner_at(sp, n, d)
+
+
+def edge_copies(n, x_ref, halo_ref, sems):
+    sp = lax.axis_index("sp")
+    tp = lax.axis_index("tp")
+    length, tile = x_ref.shape[0], halo_ref.shape[1]
+    copies = (
+        remote(x_ref.at[pl.ds(length - tile, tile)], halo_ref.at[0], sems, (0,), ((sp + 1) % n, tp)),
+        remote(x_ref.at[pl.ds(0, tile)], halo_ref.at[1], sems, (1,), ((sp + n - 1) % n, tp)),
+    )
+    for copy in copies:
+        copy.start()
+    return copies
+
+
+def halo_edges(halo, n, width):
+    sp = lax.axis_index("sp")
+    zero = jnp.zeros((), halo.dtype)
+    return (
+        jnp.where(sp == 0, zero, halo[0, halo.shape[1] - width :]),
+        jnp.where(sp == n - 1, zero, halo[1, :width]),
+    )
+
+
 def remote(src, dst, sems, index, device):
     return pltpu.make_async_remote_copy(
         src_ref=src,
@@ -100,7 +137,9 @@
     )
 
 
-def dispatch_kernel(n, sends_ref, sendi_ref, outs_ref, outi_ref, hop, pair, cross, fwd, own):
+def dispatch_kernel(
+    n, sends_ref, sendi_ref, x_ref, outs_ref, outi_ref, halo_ref, hop, pair, cross, fwd, own, edge
+):
     fourth = sends_ref.shape[2]
     sp = lax.axis_index("sp")
     tp, partner, across, _ = neighbours()
@@ -112,13 +151,14 @@
     arrays = ((sends_ref, outs_ref), (sendi_ref, outi_ref))
     greet(n)
     hops = {}
-    pending = []
+    pending = list(edge_copies(n, x_ref, halo_ref, edge))
+    away = [1] + [d for p in (0, 1) for d in range(n - 1, 1, -1) if d % 2 == p]
     for a, (src, dst) in enumerate(arrays):
         local = pltpu.make_async_copy(src.at[sp], dst.at[sp, :, mine], own.at[a])
         local.start()
         hops[a, 0] = local
-    for d in range(1, n):
-        peer = (sp + d) % n
+    for d in away:
+        peer = partner_at(sp, n, d)
         for a, (src, dst) in enumerate(arrays):
             copy = remote(src.at[peer], dst.at[sp, :, mine], hop, (a, d), (peer, tp))
             copy.start()
@@ -126,7 +166,7 @@
 
     def step_in(a, d):
         dst = arrays[a][1]
-        source = (sp + n - d) % n
+        source = source_at(sp, n, d)
         if d == 0:
             hops[a, d].wait()
         else:
@@ -141,14 +181,14 @@
 
     def step_on(a, d, over):
         dst = arrays[a][1]
-        source = (sp + n - d) % n
+        source = source_at(sp, n, d)
         over.wait_recv()
         block = dst.at[source, :, theirs]
         copy = remote(block, block, fwd, (a, d), (sp, partner))
         copy.start()
         pending.append(copy)
 
-    order = [(a, d) for d in range(n) for a in range(2)]
+    order = [(a, d) for d in [0] + away for a in range(2)]
     overs = []
     lag = 2
     for i, (a, d) in enumerate(order):
@@ -166,21 +206,21 @@
             hops[a, d].wait_send()
 
 
-def dispatch(sends, sendi, n, n_tp):
+def dispatch(sends, sendi, x, n, n_tp):
     experts, slots, fourth = sends.shape
     full = jax.ShapeDtypeStruct((experts, slots, fourth * n_tp), BF)
     dma = pltpu.SemaphoreType.DMA
     return pl.pallas_call(
         functools.partial(dispatch_kernel, n),
-        out_shape=(full, full),
-        in_specs=[VM, VM],
-        out_specs=(VM, VM),
-        scratch_shapes=[dma((2, 2, n))] * 4 + [dma((2,))],
+        out_shape=(full, full, jax.ShapeDtypeStruct((2, ROW_TILE, x.shape[1]), x.dtype)),
+        in_specs=[VM, VM, VM],
+        out_specs=(VM, VM, VM),
+        scratch_shapes=[dma((2, 2, n))] * 4 + [dma((2,)), dma((2, 2))],
         compiler_params=pltpu.CompilerParams(
             collective_id=1, has_side_effects=True, vmem_limit_bytes=40 * 2**20
         ),
         cost_estimate=pl.CostEstimate(flops=0, bytes_accessed=100_000_000, transcendentals=0),
-    )(sends, sendi)
+    )(sends, sendi, x)
 
 
 def return_kernel(
@@ -195,10 +235,10 @@
         return pl.ds(pl.multiple_of(q * fourth, 128), fourth)
 
     greet(n)
-    order = list(range(1, n)) + [0]
+    order = list(range(n - 1, -1, -1))
     pairs, crosses, hops = {}, {}, {}
     for d in order:
-        j = (sp + d) % n
+        j = partner_at(sp, n, d)
         for a, q in enumerate((diagonal, partner)):
             copy = remote(
                 part_ref.at[j, :, cols(q)], got1.at[a, j], s_pair, (a, d), (sp, partner)
@@ -207,7 +247,7 @@
             pairs[a, d] = copy
 
     def stage_b(d):
-        j = (sp + d) % n
+        j = partner_at(sp, n, d)
         pairs[0, d].wait_recv()
         total = part_ref[j, :, cols(across)].astype(F32) + got1[0, j].astype(F32)
         mid[j] = total.astype(BF)
@@ -216,7 +256,7 @@
         crosses[d] = copy
 
     def stage_c(d):
-        j = (sp + d) % n
+        j = partner_at(sp, n, d)
         pairs[1, d].wait_recv()
         crosses[d].wait_recv()
         total = part_ref[j, :, cols(tp)].astype(F32) + got1[1, j].astype(F32)
@@ -283,7 +323,11 @@
     )(part, pick)
 
 
-def exchange_kernel(n, same, src_ref, dst_ref, sems, own):
+def exchange_kernel(n, same, halo, *refs):
+    if halo:
+        src_ref, x_ref, dst_ref, halo_ref, sems, own, edge = refs
+    else:
+        src_ref, dst_ref, sems, own = refs
     sp = lax.axis_index("sp")
     tp = lax.axis_index("tp")
 
@@ -291,11 +335,11 @@
         return src_ref if same else src_ref.at[i]
 
     greet(n, with_tp=False)
+    copies = list(edge_copies(n, x_ref, halo_ref, edge)) if halo else []
     local = pltpu.make_async_copy(piece(sp), dst_ref.at[sp], own.at[0])
     local.start()
-    copies = []
-    for d in range(1, n):
-        peer = (sp + d) % n
+    for d in range(n - 1, 0, -1):
+        peer = partner_at(sp, n, d)
         copy = remote(piece(peer), dst_ref.at[sp], sems, (d,), (peer, tp))
         copy.start()
         copies.append(copy)
@@ -304,20 +348,26 @@
         copy.wait()
 
 
-def exchange(x, n, same, cid):
-    shape = (n,) + x.shape if same else x.shape
+def exchange(x, n, same, cid, edges=None):
+    out = [jax.ShapeDtypeStruct((n,) + x.shape if same else x.shape, x.dtype)]
     dma = pltpu.SemaphoreType.DMA
+    scratch = [dma((2, n)), dma((1,))]
+    args = [x]
+    if edges is not None:
+        args.append(edges)
+        out.append(jax.ShapeDtypeStruct((2, ROW_TILE, edges.shape[1]), edges.dtype))
+        scratch.append(dma((2, 2)))
     return pl.pallas_call(
-        functools.partial(exchange_kernel, n, same),
-        out_shape=jax.ShapeDtypeStruct(shape, x.dtype),
-        in_specs=[VM],
-        out_specs=VM,
-        scratch_shapes=[dma((2, n)), dma((1,))],
+        functools.partial(exchange_kernel, n, same, edges is not None),
+        out_shape=out,
+        in_specs=[VM] * len(args),
+        out_specs=[VM] * len(out),
+        scratch_shapes=scratch,
         compiler_params=pltpu.CompilerParams(
             collective_id=cid, has_side_effects=True, vmem_limit_bytes=24 * 2**20
         ),
         cost_estimate=pl.CostEstimate(flops=0, bytes_accessed=20_000_000, transcendentals=0),
-    )(x)
+    )(*args)
 
 
 def split_dot(x, w, dims):
@@ -507,14 +557,6 @@
     return full.reshape(heads * maps.shape[1], heads * maps.shape[2])
 
 
-def edge_rows(block, n, width):
-    forward = [(i, i + 1) for i in range(n - 1)]
-    backward = [(i + 1, i) for i in range(n - 1)]
-    low = lax.ppermute(block[block.shape[0] - width :], "sp", forward)
-    high = lax.ppermute(block[:width], "sp", backward)
-    return low, high
-
-
 def shards(
     cotangent,
     saved_input,
@@ -542,7 +584,6 @@
     channels = conv_input.shape[1]
     sds = jax.ShapeDtypeStruct
 
-    low, high = edge_rows(conv_input, n, 2)
     sends, sendi, pick = local_call(
         functools.partial(prepare_kernel, slots),
         (cotangent, saved_input, routes.T, route_weight.T),
@@ -552,7 +593,8 @@
             sds((experts * slots, length), BF),
         ),
     )
-    got_scaled, got_input = dispatch(sends, sendi, n, n_tp)
+    got_scaled, got_input, halo = dispatch(sends, sendi, conv_input, n, n_tp)
+    low, high = halo_edges(halo, n, 2)
     rows_scaled = got_scaled.reshape(experts * slots, width)
     rows_input = got_input.reshape(experts * slots, width)
     w_gate = gate_proj[0]
@@ -598,7 +640,7 @@
         (normed_grad, cotangent, saved_input, out_proj, gate_branch, decay, tot),
         (sds((length, width), BF), one, one, two, eight, two),
     )
-    everyone = exchange(tot2, n, True, 3)
+    (everyone,) = exchange(tot2, n, True, 3)
     conv_grad, branch_grad, mixed_out, _ = local_call(
         functools.partial(last_kernel, n),
         (
@@ -612,9 +654,11 @@
             sds((length, 4 * channels), F32),
         ),
     )
-    grad_low, grad_high = edge_rows(conv_grad, n, 2)
     grad_part = lax.dot_general(mixed_grad_b, mixed_out, rows0, preferred_element_type=F32)
-    pieces = exchange(grad_part.astype(BF).reshape(n, width // n, channels), n, False, 4)
+    pieces, grad_halo = exchange(
+        grad_part.astype(BF).reshape(n, width // n, channels), n, False, 4, conv_grad
+    )
+    grad_low, grad_high = halo_edges(grad_halo, n, 2)
     grad_out = jnp.sum(pieces.astype(F32), axis=0)
     taps32 = conv_taps.astype(F32)
     grad_pad = jnp.concatenate([grad_low, conv_grad, grad_high], axis=0).astype(F32)

time: 173 us -> 153 us (0.88)
  the two profiles are of different devices: /device:TPU:16 before, /device:TPU:0 now
where the time goes in v2:
time: 153 us; the launch traced here: 152 us
  Pallas kernels  127 us (83%)
  matrix products  12.8 us (8%)
  local copies, waits for them, and re-layouts  8.01 us (5%)
  other arithmetic  3.41 us (2%)
    pallas_call x1, Pallas kernels, dispatch(): pl.pallas_call(functools.partial(dispatch_kernel, n), out_shape=(full, fu...  48.6 us
    pallas_call x2, Pallas kernels, exchange(): pl.pallas_call(functools.partial(exchange_kernel, n, same, edges is not N...  32.6 us
    pallas_call x1, Pallas kernels, send_back(): pl.pallas_call(functools.partial(return_kernel, n), out_shape=jax.ShapeDt...  29.9 us
    pallas_call x4, Pallas kernels, local_call(): pl.pallas_call(kernel, out_shape=outs, in_specs=[VM] * len(args), out_spe...  16.1 us
    unnamed x37, local copies, waits for them, and re-layouts  7.12 us

profile of v2, /device:TPU:0, one launch (start us, length us, event | category | flops | bytes accessed | tf_op | source)
XLA Modules:
  0.0 152.3 jit_solution(15918888977095110264)
XLA Ops:
  0.6 3.2 %shard_map.190 = (bf16[8,80,512]{2,1,0:T(8,128)(2,1)}, bf16[8,80,512]{2,1,0:T(8,128)(2,1)}, bf16[640,160]{1,0:T(8,128)(2,1)}) custom-call(bf16[160,2048]{1,0:T(8,128)(2,1)} %cot_ref.3, bf16[160,2048]{1,0:T(8,128)(2,1)} %x_ref.7, s32[2,160]{1,0:T(2,128)} %bitcast.71, f32[2,160]{1,0:T(2,128)} %bitcast.72), custom_call_target="tpu_custom_call" | custom-call | flops 10000000 | bytes 4000000 | tf_op jit(solution)/shard_map/pallas_call | solution.py:20
  3.9 1.1 copy-done.2
  5.0 1.1 copy-done.3
  6.1 0.9 copy-done.6
  6.9 48.6 %shard_map.191 = (bf16[8,80,2048]{2,1,0:T(8,128)(2,1)S(1)}, bf16[8,80,2048]{2,1,0:T(8,128)(2,1)S(1)}, bf16[2,16,256]{2,1,0:T(8,128)(2,1)S(1)}) custom-call(bf16[8,80,512]{2,1,0:T(8,128)(2,1)S(1)} %copy-done.2, bf16[8,80,512]{2,1,0:T(8,128)(2,1)S(1)} %copy-done.3, bf16[160,256]{1,0:T(8,128)(2,1)S(1)} %copy-done.6), custom_call_target="tpu_custom_call" | custom-call | bytes 100000000 | tf_op jit(solution)/shard_map/pallas_call | solution.py:213
  55.5 0.8 fusion.2
  56.7 0.8 fusion.5
  58.0 1.0 multiply_convert_fusion.1
  59.0 2.3 %convolution_bitcast_fusion.2 = f32[1,2048,256]{2,1,0:T(8,128)} fusion(bf16[640,2048]{1,0:T(8,128)(2,1)S(1)} %bitcast.65, bf16[640,256]{1,0:T(8,128)(2,1)S(1)} %get-tuple-element.55), kind=kOutput, calls=%fused_computation.3 | convolution fusion | flops 671088640 | bytes 5046272 | tf_op jit(solution)/shard_map/dot_general | solution.py:623
  61.3 2.3 %convolution_bitcast_fusion.1 = f32[1,2048,256]{2,1,0:T(8,128)} fusion(bf16[640,2048]{1,0:T(8,128)(2,1)S(1)} %bitcast.66, bf16[640,256]{1,0:T(8,128)(2,1)S(1)} %get-tuple-element.54), kind=kOutput, calls=%fused_computation.2 | convolution fusion | flops 671088640 | bytes 5046272 | tf_op jit(solution)/shard_map/dot_general | solution.py:624
  63.7 2.4 %convolution_bitcast_fusion = f32[1,256,2048]{2,1,0:T(8,128)} fusion(bf16[640,2048]{1,0:T(8,128)(2,1)S(1)} %bitcast.62, f32[640,256]{1,0:T(8,128)S(1)} %fusion.5, f32[640,256]{1,0:T(8,128)S(1)} %fusion.2), kind=kOutput, calls=%fused_computation.1 | convolution fusion | flops 672071680 | bytes 6029312 | tf_op jit(solution)/shard_map/dot_general | solution.py:622
  66.0 0.9 fusion
  66.9 0.9 add_convert_fusion
  67.9 29.9 %shard_map.192.ng_ref = bf16[160,2048]{1,0:T(8,128)(2,1)S(1)} custom-call(bf16[8,80,2048]{2,1,0:T(8,128)(2,1)S(1)} %bitcast.59, bf16[640,160]{1,0:T(8,128)(2,1)S(1)} %copy-done.5), custom_call_target="tpu_custom_call" | custom-call | bytes 100000000 | tf_op jit(solution)/shard_map/pallas_call | solution.py:311
  97.8 0.8 copy-done.1
  101.6 4.6 %shard_map.193 = (f32[160,256]{1,0:T(8,128)}, f32[160,1024]{1,0:T(8,128)}, f32[2,160,256]{2,1,0:T(8,128)}, f32[2,160,256]{2,1,0:T(8,128)}, f32[2,160,256]{2,1,0:...) custom-call(bf16[160,256]{1,0:T(8,128)(2,1)} %x_ref.6, ...), custom_call_target="tpu_custom_call" | custom-call | flops 10000000 | bytes 4000000 | tf_op jit(solution)/shard_map/pallas_call | solution.py:20
  106.2 4.5 %shard_map.194 = (bf16[160,2048]{1,0:T(8,128)(2,1)}, f32[160,256]{1,0:T(8,128)}, f32[160,256]{1,0:T(8,128)}, f32[2,160,256]{2,1,0:T(8,128)}, f32[8,256]{1,0:T(8,128)}, /*index=5*/f32[2,160,256]{2,1,0:T(8,128)}) custom-call(bf16[160,2048]{1,0:T(8,128)(2,1)} %copy-done.1, bf16[160,2048]{1,0:T(8,128)(2,1)} %cot_ref.3, bf16[160,2048]{1,0:T(8,128)(2,1)} %x_ref.7, ...), custom_call_target="tpu_custom_call" | custom-call | flops 10000000 | bytes 4000000 | tf_op jit(solution)/shard_map/pallas_call | solution.py:20
  111.4 6.5 %shard_map.195.all_ref = f32[8,8,256]{2,1,0:T(8,128)S(1)} custom-call(f32[8,256]{1,0:T(8,128)S(1)} %copy-done.8), custom_call_target="tpu_custom_call" | custom-call | bytes 20000000 | tf_op jit(solution)/shard_map/pallas_call | solution.py:360
  118.6 3.7 %shard_map.196 = (bf16[160,256]{1,0:T(8,128)(2,1)}, bf16[160,256]{1,0:T(8,128)(2,1)}, bf16[160,256]{1,0:T(8,128)(2,1)}, f32[160,1024]{1,0:T(8,128)}) custom-call(f32[8,8,256]{2,1,0:T(8,128)} %copy-done.7, f32[160,256]{1,0:T(8,128)} %get-tuple-element.40.conv_ref, f32[160,1024]{1,0:T(8,128)} %get-tuple-element.41.gates_ref, ...), custom_call_target="tpu_custom_call" | custom-call | flops 10000000 | bytes 4000000 | tf_op jit(solution)/shard_map/pallas_call | solution.py:20
  122.3 1.4 convolution_convert_fusion
  123.7 0.9 copy-done.4
  124.6 26.1 %shard_map.197 = (bf16[8,256,256]{2,1,0:T(8,128)(2,1)S(1)}, bf16[2,16,256]{2,1,0:T(8,128)(2,1)S(1)}) custom-call(bf16[8,256,256]{2,1,0:T(8,128)(2,1)S(1)} %bitcast.60, bf16[160,256]{1,0:T(8,128)(2,1)S(1)} %copy-done.4), custom_call_target="tpu_custom_call" | custom-call | bytes 20000000 | tf_op jit(solution)/shard_map/pallas_call | solution.py:360
  150.7 0.8 convert_reduce_fusion
  151.6 0.7 fusion.11
  (45 shorter events, 5.1 us)
Async XLA Ops:
  0.6 54.9 %copy-start = (bf16[1,2048,256]{2,1,0:T(8,128)(2,1)S(1)}, bf16[1,2048,256]{2,1,0:T(8,128)(2,1)}, u32[]{:S(2)}) copy-start(bf16[1,2048,256]{2,1,0:T(8,128)(2,1)} %param.19) | copy-start | bytes 3145732
  3.9 1.1 copy-start.2
  5.0 1.1 copy-start.3
  6.1 0.9 copy-start.6
  55.5 1.2 copy-start.10
  56.7 1.2 copy-start.16
  66.9 1.0 copy-start.5
  67.8 31.4 %copy-start.12 = (bf16[2,4,64,64]{3,2,1,0:T(8,128)(2,1)S(1)}, bf16[2,4,64,64]{3,2,1,0:T(8,128)(2,1)}, u32[]{:S(2)}) copy-start(bf16[2,4,64,64]{3,2,1,0:T(8,128)(2,1)} %param.27) | copy-start | bytes 196612
  67.8 31.4 %copy-start.13 = (bf16[2,4,64,64]{3,2,1,0:T(8,128)(2,1)S(1)}, bf16[2,4,64,64]{3,2,1,0:T(8,128)(2,1)}, u32[]{:S(2)}) copy-start(bf16[2,4,64,64]{3,2,1,0:T(8,128)(2,1)} %param.26) | copy-start | bytes 196612
  97.8 0.9 copy-start.1
  98.6 2.1 %copy-start.15 = (f32[2,256]{1,0:T(2,128)S(1)}, f32[2,256]{1,0:T(2,128)}, u32[]{:S(2)}) copy-start(f32[2,256]{1,0:T(2,128)} %param.28) | copy-start | bytes 6148
  100.8 0.8 copy-start.9
  110.7 0.7 copy-start.8
  111.4 10.9 %copy-start.11 = (bf16[160,2048]{1,0:T(8,128)(2,1)S(1)}, bf16[160,2048]{1,0:T(8,128)(2,1)}, u32[]{:S(2)}) copy-start(bf16[160,2048]{1,0:T(8,128)(2,1)} %get-tuple-element.38) | copy-start | bytes 1966084
  118.0 0.6 copy-start.7
  122.3 29.3 %copy-start.14 = (bf16[4,256]{1,0:T(4,128)(2,1)S(1)}, bf16[4,256]{1,0:T(4,128)(2,1)}, u32[]{:S(2)}) copy-start(bf16[4,256]{1,0:T(4,128)(2,1)} %taps_ref.1) | copy-start | bytes 6148
  123.7 0.9 copy-start.4
